TPU v7x, 32 devices: a whole 2x2x4 slice. The times are simulated.
32 devices in a mesh: sp: 8 (over z, y), tp: 4 (over x, core).
Axes of the slice: x: 2, y: 2, z: 4, core: 2. Of those that a mesh axis runs over, the one named last changes fastest.
Arguments:
- mixer_input: bfloat16 [1024, 1024], P('sp', 'tp'), may hold values from -1800 to 1800
- time_step: float32 [2, 64], P(None, 'tp'), may hold values from 0 to 2, as said below
- damping: float32 [2, 1024, 64], P(None, 'sp', 'tp'), may hold values from 0 to 2
- input_map: bfloat16 [2, 2, 64, 64, 16], P(None, None, 'tp'), may hold values from -1 to 1
- readout: float32 [2, 2, 64, 16, 64], P(None, None, 'tp'), may hold values from -0.5 to 0.5
- skip_gain: float32 [1024], P('tp'), may hold values from -4 to 4
- out_gain: float32 [1024], P('tp'), may hold values from 0.1 to 1.9
- out_weight: bfloat16 [1024, 2048], replicated, may hold values from -0.1875 to 0.1875
- residual: bfloat16 [1024, 2048], P(('sp', 'tp')), may hold values from -6 to 6
- channel_gain: float32 [2048], replicated, may hold values from 0.1 to 1.9
- value_weight: bfloat16 [2048, 6144], P('sp', 'tp'), may hold values from -0.125 to 0.125
- gate_weight: bfloat16 [2048, 6144], P('sp', 'tp'), may hold values from -0.125 to 0.125
- value_taps: float32 [3, 6144], P(None, 'tp'), may hold values from -3 to 3
- gate_taps: float32 [3, 6144], P(None, 'tp'), may hold values from -3 to 3
- down_weight: bfloat16 [6144, 2048], P('tp', 'sp'), may hold values from -0.078125 to 0.078125
Outputs:
- output: bfloat16 [1024, 2048], P(('sp', 'tp'))
Inputs may be any that keep to these rules, and one draw needn't show every extreme that they name: `time_step`: positive.
All inputs are finite; a program needn't handle non-finite values.
Results may differ from a plain program's by a relative error of at most 0.017.
Values may be sent and summed in bfloat16 or wider, within the bound.
A program may use at most 128 MiB of HBM per device.

v0:
```python
import math

import jax
import jax.numpy as jnp
from jax import lax
from jax.sharding import PartitionSpec as P

norm_eps = 1e-06
highest = lax.Precision.HIGHEST


def carried_in(value, axis, join, neutral, backward):
    count, mine = (lax.axis_size(axis), lax.axis_index(axis))
    pieces = jax.tree.map(lambda part: lax.all_gather(part, axis), value)
    if backward:
        pieces = jax.tree.map(lambda part: part[::-1], pieces)
        mine = count - 1 - mine
    total = jax.tree.map(
        lambda part, zero: jnp.full_like(part, 0) + jnp.asarray(zero, part.dtype), value, neutral
    )

    def step(position, total):
        longer = join(total, jax.tree.map(lambda part: part[position], pieces))
        return jax.tree.map(lambda new, old: jnp.where(position < mine, new, old), longer, total)

    return lax.fori_loop(0, count - 1, step, total)


def with_halo(cells, sides, width):
    for axis, dim in sides:
        count = lax.axis_size(axis)
        ends = count - 1
        head = lax.slice_in_dim(cells, 0, width, axis=dim)
        tail = lax.slice_in_dim(cells, cells.shape[dim] - width, cells.shape[dim], axis=dim)
        cells = jnp.concatenate(
            [
                lax.ppermute(tail, axis, [(i, (i + 1) % count) for i in range(ends)]),
                cells,
                lax.ppermute(head, axis, [((i + 1) % count, i) for i in range(ends)]),
            ],
            axis=dim,
        )
    return cells


def combine(earlier, latter):
    prod_real = latter[0] * earlier[0] - latter[1] * earlier[1]
    prod_imag = latter[0] * earlier[1] + latter[1] * earlier[0]
    sum_real = latter[0] * earlier[2] - latter[1] * earlier[3] + latter[2]
    sum_imag = latter[0] * earlier[3] + latter[1] * earlier[2] + latter[3]
    return (prod_real, prod_imag, sum_real, sum_imag)


def moved_rows(values, offset, filler_value, backward):
    filler = jnp.full((offset, values.shape[1]), filler_value, jnp.float32)
    if backward:
        return jnp.concatenate((values[offset:], filler), axis=0)
    return jnp.concatenate((filler, values[:-offset]), axis=0)


def prefix_rows(elements, backward):
    row_count = elements[0].shape[0]
    fills = (1.0, 0.0, 0.0, 0.0)
    offset = 1
    while offset < row_count:
        earlier = tuple(
            (moved_rows(elements[index], offset, fills[index], backward) for index in range(4))
        )
        elements = combine(earlier, elements)
        offset = offset * 2
    return elements


def mixer_branch(mixer_input, time_step, damping, input_map, readout):
    tok_rows = mixer_input.shape[0]
    group_count = time_step.shape[1]
    states = input_map.shape[3]
    channels = input_map.shape[4]
    flat_width = group_count * states
    frequency = math.pi * jnp.arange(states, dtype=jnp.float32)
    ones_narrow = jnp.eye(group_count, dtype=jnp.bfloat16)
    ones_wide = jnp.eye(group_count, dtype=jnp.float32)
    sign_pair = jnp.array([1.0, -1.0], jnp.float32)
    mixed_sum = jnp.zeros((tok_rows, group_count * channels), jnp.float32)
    for direction in range(2):
        step_size = time_step[direction]
        rotation = (step_size[:, None] * frequency[None, :]).reshape(flat_width)
        in_scale = jnp.repeat(jnp.sqrt(-jnp.expm1(-step_size)), states)
        magnitude = jnp.repeat(
            jnp.exp(-0.5 * step_size[None, :] - damping[direction]), states, axis=1
        )
        decay_real = magnitude * jnp.cos(rotation)[None, :]
        decay_imag = magnitude * jnp.sin(rotation)[None, :]
        in_block = jnp.einsum("pgnh,gk->ghpkn", input_map[direction], ones_narrow).reshape(
            group_count * channels, 2 * flat_width
        )
        projected = jnp.dot(mixer_input, in_block, preferred_element_type=jnp.float32)
        drive_real = projected[:, :flat_width] * in_scale[None, :]
        drive_imag = projected[:, flat_width:] * in_scale[None, :]
        backward = direction == 1
        scanned = prefix_rows((decay_real, decay_imag, drive_real, drive_imag), backward)
        last_row = 0 if backward else tok_rows - 1
        totals = (
            scanned[0][last_row],
            scanned[1][last_row],
            scanned[2][last_row],
            scanned[3][last_row],
        )
        zero_row = jnp.zeros((flat_width,), jnp.float32)
        identity = (jnp.ones((flat_width,), jnp.float32), zero_row, zero_row, zero_row)
        carried = carried_in(totals, "sp", combine, identity, backward)
        state_real = (
            scanned[2] + scanned[0] * carried[2][None, :] - scanned[1] * carried[3][None, :]
        )
        state_imag = (
            scanned[3] + scanned[0] * carried[3][None, :] + scanned[1] * carried[2][None, :]
        )
        signed = readout[direction] * sign_pair[:, None, None, None]
        out_block = jnp.einsum("pghn,gk->pgnkh", signed, ones_wide, precision=highest).reshape(
            2 * flat_width, group_count * channels
        )
        both_parts = jnp.concatenate((state_real, state_imag), axis=1)
        mixed_sum = mixed_sum + jnp.dot(both_parts, out_block, precision=highest)
    return mixed_sum


def body(
    mixer_input,
    time_step,
    damping,
    input_map,
    readout,
    skip_gain,
    out_gain,
    out_weight,
    residual,
    channel_gain,
    value_weight,
    gate_weight,
    value_taps,
    gate_taps,
    down_weight,
):
    tok_rows, local_width = mixer_input.shape
    tp_count = lax.axis_size("tp")
    mixed_y = mixer_branch(mixer_input, time_step, damping, input_map, readout)
    mixed_y = mixed_y + skip_gain[None, :] * mixer_input.astype(jnp.float32)
    square_sum = lax.psum(jnp.sum(mixed_y * mixed_y, axis=1), "tp")
    inverse = lax.rsqrt(square_sum / (local_width * tp_count) + norm_eps)
    normed_mix = (mixed_y * inverse[:, None] * out_gain[None, :]).astype(jnp.bfloat16)
    token_block = lax.all_to_all(normed_mix, "tp", split_axis=0, concat_axis=1, tiled=True)
    mixed_rows = jnp.dot(token_block, out_weight, preferred_element_type=jnp.float32)
    hidden_state = (residual.astype(jnp.float32) + mixed_rows).astype(jnp.bfloat16)
    state_wide = hidden_state.astype(jnp.float32)
    scale_rows = lax.rsqrt(jnp.mean(state_wide * state_wide, axis=1, keepdims=True) + norm_eps)
    normed = (state_wide * scale_rows * channel_gain[None, :]).astype(jnp.bfloat16)
    block_rows = lax.all_gather(normed, "tp", axis=0, tiled=True)
    hidden_width = value_weight.shape[1]
    value_up = jnp.dot(
        block_rows,
        lax.all_gather(value_weight, "sp", axis=0, tiled=True),
        preferred_element_type=jnp.float32,
    )
    gate_up = jnp.dot(
        block_rows,
        lax.all_gather(gate_weight, "sp", axis=0, tiled=True),
        preferred_element_type=jnp.float32,
    )
    both_up = jnp.concatenate((value_up.astype(jnp.bfloat16), gate_up.astype(jnp.bfloat16)), axis=1)
    padded = with_halo(both_up, (("sp", 0),), 1)
    tap_table = jnp.concatenate((value_taps, gate_taps), axis=1)
    convolved = (
        tap_table[0] * padded[:-2].astype(jnp.float32)
        + tap_table[1] * padded[1:-1].astype(jnp.float32)
        + tap_table[2] * padded[2:].astype(jnp.float32)
    )
    hidden = (convolved[:, :hidden_width] * jax.nn.silu(convolved[:, hidden_width:])).astype(
        jnp.bfloat16
    )
    down_full = lax.all_gather(down_weight, "sp", axis=1, tiled=True)
    summed = lax.psum_scatter(
        jnp.dot(hidden, down_full, preferred_element_type=jnp.float32).astype(jnp.bfloat16),
        "tp",
        scatter_dimension=0,
        tiled=True,
    ).astype(jnp.float32)
    return (state_wide + summed).astype(jnp.bfloat16)


def solution(mesh):
    in_specs = (
        P("sp", "tp"),
        P(None, "tp"),
        P(None, "sp", "tp"),
        P(None, None, "tp", None, None),
        P(None, None, "tp", None, None),
        P("tp"),
        P("tp"),
        P(),
        P(("sp", "tp"), None),
        P(),
        P("sp", "tp"),
        P("sp", "tp"),
        P(None, "tp"),
        P(None, "tp"),
        P("tp", "sp"),
    )
    out_specs = P(("sp", "tp"), None)
    return jax.shard_map(body, mesh=mesh, in_specs=in_specs, out_specs=out_specs, check_vma=False)
```

profile of v0, /device:TPU:0, one launch (start us, length us, event | category | flops | bytes accessed | tf_op | source)
XLA Modules:
  0.0 438.9 jit_solution(8273349476924241032)
XLA Ops:
  10.7 1.8 multiply_bitcast_fusion.2
  12.5 3.4 reshape.96
  19.1 2.1 copy.38
  21.2 1.6 subtract_add_fusion.3
  27.0 1.2 fusion.32
  28.2 1.0 fusion.34
  30.0 1.4 cos.21
  31.3 1.4 sin.21
  32.7 2.4 reshape.93
  35.1 1.6 convolution_bitcast_fusion.1
  38.5 1.0 subtract_add_fusion.7
  44.5 1.0 fusion.28
  47.9 2.2 fusion.42
  50.2 1.1 fusion.45
  51.3 33.5 %all-gather.4 = f32[8,1,1024]{2,1,0:T(1,128)S(1)} all-gather(f32[1,1,1024]{2,1,0:T(1,128)S(1)} %slice_bitcast_fusion.5), channel_id=1, replica_groups=mesh['sp'=8,'tp'=4] {'sp'}, dimensions={0}, use_global_device_ids=true | all-gather | bytes 36864 | tf_op jit(solution)/shard_map/all_gather | solution.py:14
  85.4 3.9 rev.12
  89.3 31.1 %all-gather.5 = f32[8,1,1024]{2,1,0:T(1,128)S(1)} all-gather(f32[1,1,1024]{2,1,0:T(1,128)S(1)} %slice_bitcast_fusion.4), channel_id=1, replica_groups=mesh['sp'=8,'tp'=4] {'sp'}, dimensions={0}, use_global_device_ids=true | all-gather | bytes 36864 | tf_op jit(solution)/shard_map/all_gather | solution.py:14
  121.1 3.9 rev.13
  125.8 31.4 %all-gather.7 = f32[8,1,1024]{2,1,0:T(1,128)S(1)} all-gather(f32[1,1,1024]{2,1,0:T(1,128)S(1)} %slice_bitcast_fusion.2), channel_id=1, replica_groups=mesh['sp'=8,'tp'=4] {'sp'}, dimensions={0}, use_global_device_ids=true | all-gather | bytes 36864 | tf_op jit(solution)/shard_map/all_gather | solution.py:14
  157.8 3.9 rev.15
  162.5 32.2 %all-gather.6 = f32[8,1,1024]{2,1,0:T(1,128)S(1)} all-gather(f32[1,1,1024]{2,1,0:T(1,128)S(1)} %slice_bitcast_fusion.3), channel_id=1, replica_groups=mesh['sp'=8,'tp'=4] {'sp'}, dimensions={0}, use_global_device_ids=true | all-gather | bytes 36864 | tf_op jit(solution)/shard_map/all_gather | solution.py:14
  195.3 3.9 rev.14
  199.3 1.3 fusion.36
  201.1 31.2 %all-gather.3 = f32[8,1,1024]{2,1,0:T(1,128)S(1)} all-gather(f32[1,1,1024]{2,1,0:T(1,128)S(1)} %slice_bitcast_fusion.6), channel_id=1, replica_groups=mesh['sp'=8,'tp'=4] {'sp'}, dimensions={0}, use_global_device_ids=true | all-gather | bytes 36864 | tf_op jit(solution)/shard_map/all_gather | solution.py:14
  232.3 31.5 %all-gather.1 = f32[8,1,1024]{2,1,0:T(1,128)S(1)} all-gather(f32[1,1,1024]{2,1,0:T(1,128)S(1)} %slice_bitcast_fusion.8), channel_id=1, replica_groups=mesh['sp'=8,'tp'=4] {'sp'}, dimensions={0}, use_global_device_ids=true | all-gather | bytes 36864 | tf_op jit(solution)/shard_map/all_gather | solution.py:14
  263.8 33.0 %all-gather = f32[8,1,1024]{2,1,0:T(1,128)S(1)} all-gather(f32[1,1,1024]{2,1,0:T(1,128)S(1)} %slice_bitcast_fusion.9), channel_id=1, replica_groups=mesh['sp'=8,'tp'=4] {'sp'}, dimensions={0}, use_global_device_ids=true | all-gather | bytes 36864 | tf_op jit(solution)/shard_map/all_gather | solution.py:14
  296.9 35.1 %all-gather.2 = f32[8,1,1024]{2,1,0:T(1,128)S(1)} all-gather(f32[1,1,1024]{2,1,0:T(1,128)S(1)} %slice_bitcast_fusion.7), channel_id=1, replica_groups=mesh['sp'=8,'tp'=4] {'sp'}, dimensions={0}, use_global_device_ids=true | all-gather | bytes 36864 | tf_op jit(solution)/shard_map/all_gather | solution.py:14
  332.4 4.5 %multiply_bitcast_fusion = (f32[2,16,64,16,16]{2,1,0,4,3:T(8,128)}, f32[2,16,64,16,16]{2,1,0,4,3:T(8,128)}) fusion(f32[16,2,16,64]{3,0,1,2:T(8,128)S(1)} %copy.41, f32[16,16]{0,1:T(8,128)S(1)} %copy-done.21, f32[16,2,16,64]{3,0,1,2:T(8,128)S(1)} %copy.37), kind=kLoop, calls=%fused_computation.12 | loop fusion | flops 1048576 | bytes 4457472 | tf_op jit(solution)/shard_map/pghn,gk->pgnkh/transpose | solution.py:119
  336.8 5.2 %reshape.94 = f32[2048,256]{0,1:T(8,128)} reshape(f32[2,16,64,16,16]{2,1,0,4,3:T(8,128)} %get-tuple-element.455) | data formatting | bytes 4194304 | tf_op jit(solution)/shard_map/reshape | solution.py:119
  342.1 3.7 reshape.97
  346.3 1.6 multiply_subtract_fusion.5
  348.2 2.2 fusion.3
  350.5 11.4 %while.33 = (s32[]{:T(128)}, f32[1024]{0:T(1024)S(1)}, f32[1024]{0:T(1024)S(1)}, s32[]{:T(128)}, f32[8,1024]{1,0:T(8,128)}, /*index=5*/f32[8,1024]{1,0:T(8,128)}...) while((s32[]{:T(128)}, f32[1024]{0:T(1024)S(1)}, f32[1024]{0:T(1024)S(1)}, ...), condition=%wide.region_3.4_spmd.clone, body=%wide.region_2.3_spmd.clone.sunk | while | flops 12292 | bytes 65665 | solution.py:26
  361.9 1.4 multiply_subtract_fusion
  363.3 2.3 multiply_reduce_fusion.1
  365.7 5.8 %psum.7 = f32[128]{0:T(128)S(1)} all-reduce(f32[128]{0:T(128)S(1)} %get-tuple-element.470), channel_id=1, replica_groups=mesh['sp'=8,'tp'=4] {'tp'}, use_global_device_ids=true, to_apply=%region_5.6 | all-reduce | flops 128 | bytes 1024 | tf_op jit(solution)/shard_map/psum | solution.py:148
  372.1 3.3 all-to-all-start
  375.5 4.0 all-to-all-done
  379.5 3.1 multiply_reduce_fusion
  382.8 6.6 %all_gather.44 = bf16[128,2048]{1,0:T(8,128)(2,1)S(1)} all-gather(bf16[32,2048]{1,0:T(8,128)(2,1)S(1)} %multiply_convert_fusion), channel_id=1, replica_groups=mesh['sp'=8,'tp'=4] {'tp'}, dimensions={0}, use_global_device_ids=true | all-gather | bytes 655360 | tf_op jit(solution)/shard_map/all_gather | solution.py:157
  389.4 3.8 convolution_convert_fusion.1
  393.2 3.8 convolution_convert_fusion.2
  397.0 1.3 collective-permute-start
  398.3 1.3 collective-permute-start.1
  399.7 4.2 collective-permute-done.1
  404.5 4.6 %convolution_convert_fusion = bf16[128,2048]{1,0:T(8,128)(2,1)} fusion(bf16[1536,2048]{1,0:T(8,128)(2,1)} %all-gather.16.cloned.1.call-done, f32[128,3072]{1,0:T(8,128)S(1)} %multiply_add_fusion), kind=kOutput, calls=%fused_computation.16 | convolution fusion | flops 806748160 | bytes 8388608 | tf_op jit(solution)/shard_map/dot_general | solution.py:182
  409.1 21.7 %reduce-scatter.2.cloned.1.call-done = bf16[32,2048]{1,0:T(8,128)(2,1)} async-done(((bf16[128,2048]{1,0:T(8,128)(2,1)}), bf16[32,2048]{1,0:T(8,128)(2,1)}) %reduce-scatter.2.cloned.1.call-update) | async-done | bytes 131088 | tf_op jit(solution)/shard_map/reduce_scatter | solution.py:181
  430.8 1.6 add_convert_fusion
  (237 shorter events, 39.7 us)
Async XLA Ops:
  6.5 2.2 copy-start.26
  6.5 3.7 copy-start.19
  6.5 382.8 %all-gather.14.cloned.1.call-start = ((), (), s32[]{:S(2)}) async-start(), calls=%async_computation.3 | async-start | bytes 7077888 | tf_op jit(solution)/shard_map/all_gather | solution.py:166
  7.3 385.9 %all-gather.12.cloned.1.call-start = ((), (), s32[]{:S(2)}) async-start(), calls=%async_computation.2 | async-start | bytes 7077888 | tf_op jit(solution)/shard_map/all_gather | solution.py:161
  8.0 396.5 %all-gather.16.cloned.1.call-start = ((), (), s32[]{:S(2)}) async-start(), calls=%async_computation.4 | async-start | bytes 7077888 | tf_op jit(solution)/shard_map/all_gather | solution.py:180
  12.5 3.6 copy-start.16
  16.4 1.8 copy-start.24
  16.5 0.8 copy-start.2
  21.2 1.7 copy-start.1
  21.2 1.7 copy-start.3
  35.1 1.6 copy-start.27
  44.5 3.4 copy-start.4
  47.9 2.2 copy-start.5
  50.2 149.1 %copy-start.6 = (f32[128,1024]{1,0:T(8,128)S(1)}, f32[128,1024]{1,0:T(8,128)}, u32[]{:S(2)}) copy-start(f32[128,1024]{1,0:T(8,128)} %fusion.28) | copy-start | bytes 1572868
  50.2 149.2 %copy-start.15 = (f32[96,1024]{1,0:T(8,128)S(1)}, f32[96,1024]{1,0:T(8,128)}, u32[]{:S(2)}) copy-start(f32[96,1024]{1,0:T(8,128)} %slice.352) | copy-start | bytes 1179652
  51.3 148.0 %copy-start.10 = (f32[128,1024]{1,0:T(8,128)}, f32[128,1024]{1,0:T(8,128)S(1)}, u32[]{:S(2)}) copy-start(f32[128,1024]{1,0:T(8,128)S(1)} %get-tuple-element.429) | copy-start | bytes 1572868
  51.3 148.0 %copy-start.12 = (f32[128,1024]{1,0:T(8,128)}, f32[128,1024]{1,0:T(8,128)S(1)}, u32[]{:S(2)}) copy-start(f32[128,1024]{1,0:T(8,128)S(1)} %get-tuple-element.430) | copy-start | bytes 1572868
  200.6 96.2 %copy-start.8 = (f32[128,1024]{1,0:T(8,128)}, f32[128,1024]{1,0:T(8,128)S(1)}, u32[]{:S(2)}) copy-start(f32[128,1024]{1,0:T(8,128)S(1)} %get-tuple-element.396) | copy-start | bytes 1572868
  200.7 131.3 %copy-start.18 = (f32[2,2,16,16,64]{4,3,2,1,0:T(8,128)S(1)}, f32[2,2,16,16,64]{4,3,2,1,0:T(8,128)}, u32[]{:S(2)}) copy-start(f32[2,2,16,16,64]{4,3,2,1,0:T(8,128)} %param.24) | copy-start | bytes 786436
  200.7 131.3 %copy-start.30 = (f32[2]{0:T(128)S(1)}, f32[2]{0:T(128)}, u32[]{:S(2)}) copy-start(f32[2]{0:T(128)} %constant.89.clone) | copy-start | bytes 28
  201.0 135.8 %copy-start.13 = (f32[128,1024]{1,0:T(8,128)}, f32[128,1024]{1,0:T(8,128)S(1)}, u32[]{:S(2)}) copy-start(f32[128,1024]{1,0:T(8,128)S(1)} %get-tuple-element.432) | copy-start | bytes 1572868
  201.0 135.8 %copy-start.14 = (f32[128,1024]{1,0:T(8,128)}, f32[128,1024]{1,0:T(8,128)S(1)}, u32[]{:S(2)}) copy-start(f32[128,1024]{1,0:T(8,128)S(1)} %get-tuple-element.442) | copy-start | bytes 1572868
  201.0 131.3 %copy-start.21 = (f32[16,16]{0,1:T(8,128)S(1)}, f32[16,16]{0,1:T(8,128)}, u32[]{:S(2)}) copy-start(f32[16,16]{0,1:T(8,128)} %fusion.55) | copy-start | bytes 3076
  342.1 4.2 copy-start.9
  346.3 1.9 copy-start
  347.9 14.0 %copy-start.7 = (f32[128,1024]{1,0:T(8,128)S(1)}, f32[128,1024]{1,0:T(8,128)}, u32[]{:S(2)}) copy-start(f32[128,1024]{1,0:T(8,128)} %get-tuple-element.375) | copy-start | bytes 1572868
  347.9 14.0 %copy-start.11 = (f32[128,1024]{1,0:T(8,128)S(1)}, f32[128,1024]{1,0:T(8,128)}, u32[]{:S(2)}) copy-start(f32[128,1024]{1,0:T(8,128)} %copy-done.10) | copy-start | bytes 1572868
  350.4 12.9 %copy-start.17 = (bf16[128,256]{1,0:T(8,128)(2,1)S(1)}, bf16[128,256]{1,0:T(8,128)(2,1)}, u32[]{:S(2)}) copy-start(bf16[128,256]{1,0:T(8,128)(2,1)} %param.20) | copy-start | bytes 196612
  350.4 12.9 %copy-start.28 = (f32[256]{0:T(256)S(1)}, f32[256]{0:T(256)}, u32[]{:S(2)}) copy-start(f32[256]{0:T(256)} %param.25) | copy-start | bytes 3076
  363.3 8.2 %copy-start.29 = (f32[256]{0:T(256)S(1)}, f32[256]{0:T(256)}, u32[]{:S(2)}) copy-start(f32[256]{0:T(256)} %param.26) | copy-start | bytes 3076
  363.3 12.2 %copy-start.22 = (f32[3,1536]{1,0:T(4,128)S(1)}, f32[3,1536]{1,0:T(4,128)}, u32[]{:S(2)}) copy-start(f32[3,1536]{1,0:T(4,128)} %param.32) | copy-start | bytes 55300
  363.3 12.2 %copy-start.23 = (f32[3,1536]{1,0:T(4,128)S(1)}, f32[3,1536]{1,0:T(4,128)}, u32[]{:S(2)}) copy-start(f32[3,1536]{1,0:T(4,128)} %param.33) | copy-start | bytes 55300
  363.3 16.2 %copy-start.20 = (bf16[32,2048]{1,0:T(8,128)(2,1)S(1)}, bf16[32,2048]{1,0:T(8,128)(2,1)}, u32[]{:S(2)}) copy-start(bf16[32,2048]{1,0:T(8,128)(2,1)} %param.28) | copy-start | bytes 393220
  372.1 7.4 %all-to-all-start = ((bf16[4,32,256]{2,1,0:T(8,128)(2,1)}), bf16[4,32,256]{2,1,0:T(8,128)(2,1)S(1)}, u32[]{:S(2)}, u32[]{:S(2)}) async-start(bf16[4,32,256]{2,1,0:T(8,128)(2,1)} %bitcast.30), calls=%async_computation | async-start | bytes 131072 | tf_op jit(solution)/shard_map/all_to_all | solution.py:151
  375.4 55.4 %reduce-scatter.2.cloned.1.call-start = ((), (), s32[]{:S(2)}) async-start(), calls=%async_computation.5 | async-start | bytes 655360 | tf_op jit(solution)/shard_map/reduce_scatter | solution.py:181
  379.5 3.2 copy-start.25
  397.0 2.7 collective-permute-start
  398.3 5.6 %collective-permute-start.1 = (bf16[1,3072]{1,0:T(2,128)(2,1)S(1)}, bf16[1,3072]{1,0:T(2,128)(2,1)S(1)}, u32[]{:S(2)}, u32[]{:S(2)}) collective-permute-start(bf16[1,3072]{1,0:T(2,128)(2,1)S(1)} %get-tuple-element.444), channel_id=1, source_target_pairs={{4,0},{8,4},{12,8},{16,12},{20,16},{24,20},{28,24},{5,1},{9,5},{13... | collective-permute-start | bytes 18440 | tf_op jit(solution)/shard_map/ppermute | solution.py:39
Sparse Core Ops, SparseCore 0:
  9.5 102.3 all-gather.13
  114.1 97.8 all-gather.11
  214.0 98.5 all-gather.15
  409.3 21.5 reduce-scatter.1
where the time goes:
time: 442 us; the launch traced here: 439 us
  blocking collectives  271 us (61%)
  local copies, waits for them, and re-layouts  60 us (14%)
  other arithmetic  33 us (7%)
  waiting for transfers between devices  32.1 us (7%)
  matrix products  21.7 us (5%)
  between operations  14.2 us (3%)
  starting transfers between devices  5.99 us (1%)
    all_gather x8, blocking collectives, carried_in(): pieces = jax.tree.map(lambda part: lax.all_gather(part, axis), value)  259 us
    reduce_scatter x1, waiting for transfers between devices, body(): lax.psum_scatter(jnp.dot(hidden, down_full, preferred_element_type=jnp.fl...  21.7 us
    rev x4, local copies, waits for them, and re-layouts, carried_in(): pieces = jax.tree.map(lambda part: part[::-1], pieces)  15.8 us
    add x14, other arithmetic, combine(): sum_real = latter[0] * earlier[2] - latter[1] * earlier[3] + latter[2]  11.8 us
    dynamic_slice x28, local copies, waits for them, and re-layouts, step(): longer = join(total, jax.tree.map(lambda part: part[position], pieces))  11.2 us
    reshape x2, local copies, waits for them, and re-layouts, mixer_branch(): jnp.einsum('pghn,gk->pgnkh', signed, ones_wide, precision=highest)  8.88 us
  transfers between devices with their start and end apart: 7, of which 4 were waited for; matrix products, arithmetic and copies ran while one was open for 24% of the time, Pallas kernels for 0%

commit v1 on v0

v1 whole, which is shorter than its diff:
```python
import math

import jax
import jax.numpy as jnp
from jax import lax
from jax.sharding import PartitionSpec as P

norm_eps = 1e-06
highest = lax.Precision.HIGHEST


def turns(step_size, count):
    coarse = jnp.round(step_size * 1024.0) / 1024.0
    whole = coarse * count
    whole = whole - 2.0 * jnp.floor(whole * 0.5)
    return whole + (step_size - coarse) * count


def mixer(mixer_input, time_step, damping, input_map, readout, skip_gain):
    rows = mixer_input.shape[0]
    groups = time_step.shape[1]
    states, width = input_map.shape[3], input_map.shape[4]
    count, mine = lax.axis_size("sp"), lax.axis_index("sp")
    at = jnp.arange(rows)
    lower = at[:, None] >= at[None, :]
    reach = jnp.stack((lower, lower.T))
    log_decay = -0.5 * time_step[:, None, :] - damping
    log_sum = jnp.einsum("ktu,kug->kgt", reach.astype(jnp.float32), log_decay, precision=highest)
    weights = jnp.where(
        reach[:, None],
        jnp.exp(jnp.minimum(log_sum[:, :, :, None] - log_sum[:, :, None, :], 0.0)),
        0.0,
    )
    number = jnp.arange(states, dtype=jnp.float32)
    dt = time_step[:, :, None, None]
    angle = math.pi * turns(dt, number[None, :] * at.astype(jnp.float32)[:, None])
    sign = jnp.array([1.0, -1.0], jnp.float32)[:, None, None, None]
    cos, sin = jnp.cos(angle), jnp.sin(angle) * sign
    grouped = mixer_input.reshape(rows, groups, width)
    drive = jnp.einsum("tgh,kpgnh->kpgtn", grouped, input_map, preferred_element_type=jnp.float32)
    drive = drive * jnp.sqrt(-jnp.expm1(-time_step))[:, None, :, None, None]
    rotated = jnp.concatenate(
        (cos * drive[:, 0] + sin * drive[:, 1], cos * drive[:, 1] - sin * drive[:, 0]), axis=3
    )
    local = jnp.einsum("kgts,kgsn->kgtn", weights, rotated, precision=highest)
    ends = jnp.stack((local[0, :, -1], local[1, :, 0]))
    totals = jnp.stack((log_sum[0, :, -1], log_sum[1, :, 0]))
    packed = jnp.concatenate((ends, jnp.repeat(totals[:, :, None], 128, axis=2)), axis=2)
    every = lax.all_gather(packed, "sp")
    end_all, total_all = every[..., : 2 * states], every[..., 2 * states]
    index = jnp.arange(count)
    away = jnp.stack((mine - index, index - mine), axis=1)
    lo = jnp.minimum(index, mine)[:, None]
    hi = jnp.maximum(index, mine)[:, None]
    between = ((index[None, :] > lo) & (index[None, :] < hi)).astype(jnp.float32)
    span = jnp.einsum("ji,ikg->jkg", between, total_all, precision=highest)
    factor = jnp.where(away[:, :, None] > 0, jnp.exp(span), 0.0)
    block_turn = turns(time_step[:, :, None], number * rows)
    hop = jnp.abs(mine - index).astype(jnp.float32)[:, None, None, None] * block_turn
    hop = math.pi * (hop - 2.0 * jnp.floor(hop * 0.5))
    hop_cos, hop_sin = jnp.cos(hop) * factor[..., None], jnp.sin(hop) * factor[..., None]
    end_re, end_im = end_all[..., :states], end_all[..., states:]
    carry = jnp.concatenate(
        (
            jnp.sum(hop_cos * end_re - hop_sin * end_im, axis=0),
            jnp.sum(hop_cos * end_im + hop_sin * end_re, axis=0),
        ),
        axis=2,
    )
    local = local + jnp.exp(log_sum)[..., None] * carry[:, :, None, :]
    re, im = local[..., :states], local[..., states:]
    state = jnp.concatenate((cos * re - sin * im, cos * im + sin * re), axis=3)
    out_map = jnp.concatenate((readout[:, 0], -readout[:, 1]), axis=3)
    mixed = jnp.einsum("kgtn,kghn->tgh", state, out_map, precision=highest)
    return mixed.reshape(rows, groups * width) + skip_gain[None, :] * mixer_input.astype(
        jnp.float32
    )


def body(
    mixer_input,
    time_step,
    damping,
    input_map,
    readout,
    skip_gain,
    out_gain,
    out_weight,
    residual,
    channel_gain,
    value_weight,
    gate_weight,
    value_taps,
    gate_taps,
    down_weight,
):
    count, mine = lax.axis_size("sp"), lax.axis_index("sp")
    depth, hidden_width = value_weight.shape
    part = hidden_width // count
    up_send = jnp.concatenate(
        (
            value_weight.reshape(depth, count, part).swapaxes(0, 1),
            gate_weight.reshape(depth, count, part).swapaxes(0, 1),
        ),
        axis=2,
    )
    up_all = lax.all_to_all(up_send, "sp", split_axis=0, concat_axis=0, tiled=True)
    up_all = up_all.reshape(count * depth, 2 * part)
    down_send = down_weight.reshape(count, part, down_weight.shape[1])
    down_all = lax.all_to_all(down_send, "sp", split_axis=0, concat_axis=0, tiled=True)
    gain = lax.all_gather(out_gain, "tp", axis=0, tiled=True)
    mixed_y = mixer(mixer_input, time_step, damping, input_map, readout, skip_gain)
    mixed_y = lax.all_to_all(mixed_y, "tp", split_axis=0, concat_axis=1, tiled=True)
    inverse = lax.rsqrt(jnp.mean(mixed_y * mixed_y, axis=1, keepdims=True) + norm_eps)
    normed_mix = (mixed_y * inverse * gain[None, :]).astype(jnp.bfloat16)
    mixed_rows = jnp.dot(normed_mix, out_weight, preferred_element_type=jnp.float32)
    hidden_state = (residual.astype(jnp.float32) + mixed_rows).astype(jnp.bfloat16)
    state_wide = hidden_state.astype(jnp.float32)
    scale_rows = lax.rsqrt(jnp.mean(state_wide * state_wide, axis=1, keepdims=True) + norm_eps)
    normed = (state_wide * scale_rows * channel_gain[None, :]).astype(jnp.bfloat16)
    rows_all = lax.all_gather(normed, ("sp", "tp"), axis=0, tiled=True)
    up = jnp.dot(rows_all, up_all, preferred_element_type=jnp.float32)
    up = up.astype(jnp.bfloat16).astype(jnp.float32)
    taps = jnp.concatenate(
        (
            lax.dynamic_slice_in_dim(value_taps, mine * part, part, axis=1),
            lax.dynamic_slice_in_dim(gate_taps, mine * part, part, axis=1),
        ),
        axis=1,
    )
    padded = jnp.pad(up, ((1, 1), (0, 0)))
    convolved = taps[0] * padded[:-2] + taps[1] * padded[1:-1] + taps[2] * padded[2:]
    hidden = (convolved[:, :part] * jax.nn.silu(convolved[:, part:])).astype(jnp.bfloat16)
    partial = jnp.einsum("tf,sfd->tsd", hidden, down_all, preferred_element_type=jnp.float32)
    partial = partial.astype(jnp.bfloat16).reshape(hidden.shape[0], -1)
    summed = lax.psum_scatter(partial, ("sp", "tp"), scatter_dimension=0, tiled=True)
    return (state_wide + summed.astype(jnp.float32)).astype(jnp.bfloat16)


def solution(mesh):
    in_specs = (
        P("sp", "tp"),
        P(None, "tp"),
        P(None, "sp", "tp"),
        P(None, None, "tp", None, None),
        P(None, None, "tp", None, None),
        P("tp"),
        P("tp"),
        P(),
        P(("sp", "tp"), None),
        P(),
        P("sp", "tp"),
        P("sp", "tp"),
        P(None, "tp"),
        P(None, "tp"),
        P("tp", "sp"),
    )
    out_specs = P(("sp", "tp"), None)
    return jax.shard_map(body, mesh=mesh, in_specs=in_specs, out_specs=out_specs, check_vma=False)
```

time: 442 us -> 321 us (0.73)
  blocking collectives: 271 us -> 89.2 us
  waiting for transfers between devices: 32.1 us -> 160 us
  local copies, waits for them, and re-layouts: 60 us -> 14 us
  other arithmetic: 33 us -> 15.9 us
    all_gather x9 -> x2, blocking collectives: 266 us -> 37.9 us  [the longest x1 32.5 us: mixer(): every = lax.all_gather(packed, 'sp')]
    reduce_scatter x1, waiting for transfers between devices: 21.7 us -> 142 us  [body(): lax.psum_scatter(partial, ('sp', 'tp'), scatter_dimension=0, tiled=True)]
    all_to_all x0 -> x1, blocking collectives: none -> 51.3 us  [body(): lax.all_to_all(up_send, 'sp', split_axis=0, concat_axis=0, tiled=True)]
    rev x4 -> x0, local copies, waits for them, and re-layouts: 15.8 us -> none  [carried_in(): pieces = jax.tree.map(lambda part: part[::-1], pieces)]
    all_gather x3 -> x1, waiting for transfers between devices: 0.04 us -> 14.5 us  [body(): rows_all = lax.all_gather(normed, ('sp', 'tp'), axis=0, tiled=True)]
    dynamic_slice x28 -> x1, local copies, waits for them, and re-layouts: 11.2 us -> 0.79 us  [body(): lax.dynamic_slice_in_dim(gate_taps, mine * part, part, axis=1)]
    reshape x6 -> x3, local copies, waits for them, and re-layouts: 17 us -> 6.69 us  [the longest x1 6.52 us: body(): partial = partial.astype(jnp.bfloat16).reshape(hidden.shape[0], -1)]
    add x27 -> x5, other arithmetic: 16.7 us -> 7.22 us  [the longest x1 4.5 us: mixer(): cos * drive[:, 0] + sin * drive[:, 1]]
  transfers between devices with their start and end apart: 7 -> 4, of which waited for: 4 -> 3; matrix products, arithmetic and copies ran while one was open for 24% -> 2% of each run, Pallas kernels for 0% -> 0%
where the time goes in v1:
time: 321 us
  waiting for transfers between devices  160 us (50%)
  blocking collectives  89.2 us (28%)
  matrix products  20.1 us (6%)
  other arithmetic  15.9 us (5%)
  local copies, waits for them, and re-layouts  14 us (4%)
  between operations  13.8 us (4%)
  starting transfers between devices  7.8 us (2%)
    reduce_scatter x1, waiting for transfers between devices, body(): lax.psum_scatter(partial, ('sp', 'tp'), scatter_dimension=0, tiled=True)  142 us
    all_to_all x1, blocking collectives, body(): lax.all_to_all(up_send, 'sp', split_axis=0, concat_axis=0, tiled=True)  51.3 us
    all_gather x1, blocking collectives, mixer(): every = lax.all_gather(packed, 'sp')  32.5 us
    all_gather x1, waiting for transfers between devices, body(): rows_all = lax.all_gather(normed, ('sp', 'tp'), axis=0, tiled=True)  14.5 us
    reshape x1, local copies, waits for them, and re-layouts, body(): partial = partial.astype(jnp.bfloat16).reshape(hidden.shape[0], -1)  6.52 us
  transfers between devices with their start and end apart: 4, of which 3 were waited for; matrix products, arithmetic and copies ran while one was open for 2% of the time, Pallas kernels for 0%

profile of v1, /device:TPU:0, one launch (start us, length us, event | category | flops | bytes accessed | tf_op | source)
XLA Modules:
  0.0 320.5 jit_solution(13191322508851586775)
XLA Ops:
  6.6 0.7 broadcast_multiply_fusion
  7.3 0.1 copy.80
  7.4 0.1 copy.79
  7.5 0.1 copy.83
  7.6 1.0 fusion.64
  8.6 0.2 slice_reduce_fusion.1
  8.8 1.0 copy.81
  9.7 1.5 bitcast_multiply_fusion
  11.2 4.5 %multiply_add_fusion.2 = (f32[2,16,128,64]{2,3,0,1:T(8,128)S(1)}, f32[2,16,128,64]{2,3,0,1:T(8,128)S(1)}) fusion(f32[2,2,16,128,64]{3,4,1,0,2:T(8,128)S(1)} %bitcast_multiply_fusion, f32[2]{0:T(128)S(1)} %copy-done.7, f32[2,16]{0,1:T(8,128)S(1)} %copy.80, f32[128,64]{0,1:T(8,128)S(1)} %iota_multiply_fusion, f32[2,16]{0,1:T(8,128)S(1)} %copy.79), kind=kLoop, calls=%fused_computation.39 | loop fusion | flops 3932160 | bytes 4227336 | tf_op jit(solution)/shard_map/add | solution.py:43
  15.7 4.6 %fusion.6 = f32[2,16,128,128]{3,2,1,0:T(8,128)S(1)} fusion(f32[2,16,128]{2,1,0:T(8,128)S(1)} %get-tuple-element.25, pred[2,128,128]{2,1,0:T(8,128)(4,1)S(1)} %pad_add_fusion, f32[2,16,128,64]{2,3,0,1:T(8,128)S(1)} %get-tuple-element.15, f32[2,16,128,64]{2,3,0,1:T(8,128)S(1)} %get-tuple-element.14), kind=kOutput, calls=%fused_computation.9 | convolution fusion | flops 807403520 | bytes 4243456 | tf_op jit(solution)/shard_map/kgts,kgsn->kgtn/dot_general | solution.py:45
  20.4 1.3 copy-done
  21.7 2.0 copy.91
  23.7 0.1 fusion.47
  23.9 0.1 reshape.178
  24.0 32.5 %all-gather = f32[16,16,256]{2,1,0:T(8,128)S(1)} all-gather(f32[2,16,256]{2,1,0:T(8,128)S(1)} %pad_maximum_fusion.2), channel_id=2, replica_groups=mesh['sp'=8,'tp'=4] {'sp'}, dimensions={0}, use_global_device_ids=true | all-gather | bytes 294912 | tf_op jit(solution)/shard_map/all_gather | solution.py:49
  56.5 0.2 copy.109
  56.7 0.2 fusion.17
  56.9 0.6 subtract_reduce_fusion
  57.5 0.1 pad_maximum_fusion.3
  57.6 0.7 multiply_add_fusion
  58.4 4.5 %multiply_subtract_fusion.1 = (f32[2,16,128,64]{2,3,0,1:T(8,128)S(1)}, f32[2,16,128,64]{2,3,0,1:T(8,128)S(1)}) fusion(f32[2,16,128,128]{2,3,0,1:T(8,128)S(1)} %multiply_add_fusion, f32[2]{0:T(128)S(1)} %copy-done.7, f32[2,16]{0,1:T(8,128)S(1)} %copy.80, f32[128,64]{0,1:T(8,128)S(1)} %iota_multiply_fusion, f32[2,16]{0,1:T(8,128)S(1)} %copy.79), kind=kLoop, calls=%fused_computation.37 | loop fusion | flops 3932160 | bytes 4227336 | tf_op jit(solution)/shard_map/sub | solution.py:72
  62.9 0.1 fusion.33
  63.0 1.2 fusion.2
  64.2 0.1 copy.93
  64.3 0.7 multiply_add_fusion.3
  65.0 3.3 %all-to-all-start = ((f32[4,32,256]{2,1,0:T(8,128)}), f32[4,32,256]{2,1,0:T(8,128)S(1)}, u32[]{:S(2)}, u32[]{:S(2)}) async-start(f32[4,32,256]{2,1,0:T(8,128)} %bitcast.17), calls=%async_computation | async-start | bytes 262144 | tf_op jit(solution)/shard_map/all_to_all | solution.py:113
  68.3 5.4 %all-gather.1 = f32[4,1,256]{2,1,0:T(1,128)S(1)} all-gather(f32[1,1,256]{2,1,0:T(1,128)S(1)} %bitcast.85), channel_id=1, replica_groups=mesh['sp'=8,'tp'=4] {'tp'}, dimensions={0}, use_global_device_ids=true | all-gather | bytes 5120 | tf_op jit(solution)/shard_map/all_gather | solution.py:111
  73.7 0.1 fusion.42
  73.9 3.2 %multiply_reduce_fusion = (f32[32]{0:T(128)S(1)}, f32[32,2048]{1,0:T(8,128)S(1)}) fusion(bf16[1024,2048]{1,0:T(8,128)(2,1)} %param.23, f32[32,1024]{1,0:T(8,128)S(1)} %bitcast.77, f32[1024]{0:T(1024)S(1)} %bitcast.82, f32[32]{0:T(128)S(1)} %add_rsqrt_fusion.1, bf16[32,2048]{1,0:T(8,128)(2,1)S(1)} %copy-done.5), kind=kOutput, calls=%fused_computation.58 | convolution fusion | flops 134709216 | bytes 4722944 | tf_op jit(solution)/shard_map/dot_general | solution.py:116
  77.2 0.7 multiply_convert_fusion
  78.0 0.3 copy.95
  78.3 0.1 copy-done.2
  78.4 0.3 copy.96
  78.6 0.1 pad_maximum_fusion.1
  78.8 51.3 %all_to_all.29 = bf16[8,256,384]{1,2,0:T(8,128)(2,1)S(1)} all-to-all(bf16[8,256,384]{1,2,0:T(8,128)(2,1)S(1)} %pad_maximum_fusion.1), channel_id=1, replica_groups=mesh['sp'=8,'tp'=4] {'sp'}, dimensions={0} | all-to-all | bytes 3145728 | tf_op jit(solution)/shard_map/all_to_all | solution.py:107
  130.0 4.2 %all-to-all-start.2 = ((bf16[8,192,256]{2,1,0:T(8,128)(2,1)}), bf16[8,192,256]{2,1,0:T(8,128)(2,1)}, u32[]{:S(2)}, u32[]{:S(2)}) async-start(bf16[8,192,256]{2,1,0:T(8,128)(2,1)} %bitcast.27), calls=%async_computation.2 | async-start | bytes 1572864 | tf_op jit(solution)/shard_map/all_to_all | solution.py:110
  134.2 0.2 reduce-scatter.2.cloned.1.call-start
  134.5 0.8 constant_dynamic-slice_fusion
  135.3 0.1 maximum_reduce_fusion.1
  135.4 0.9 copy.97
  136.2 14.5 %all-gather.4.cloned.1.call-done = bf16[1024,2048]{1,0:T(8,128)(2,1)} async-done(((bf16[32,2048]{1,0:T(8,128)(2,1)}), bf16[1024,2048]{1,0:T(8,128)(2,1)}) %all-gather.4.cloned.1.call-update) | async-done | bytes 4194320 | tf_op jit(solution)/shard_map/all_gather | solution.py:121
  150.7 4.0 %fusion.16 = f32[1024,384]{0,1:T(8,128)S(1)} fusion(bf16[1024,2048]{1,0:T(8,128)(2,1)} %all-gather.4.cloned.1.call-done, bf16[2048,384]{1,0:T(8,128)(2,1)S(1)} %bitcast.75), kind=kOutput, calls=%fused_computation.27 | convolution fusion | flops 1611399168 | bytes 7340032 | tf_op jit(solution)/shard_map/dot_general | solution.py:122
  154.7 1.3 fusion.14
  156.0 3.4 %all-to-all-done.2 = bf16[8,192,256]{2,1,0:T(8,128)(2,1)} async-done(((bf16[8,192,256]{2,1,0:T(8,128)(2,1)}), bf16[8,192,256]{2,1,0:T(8,128)(2,1)}, u32[]{:S(2)}, u32[]{:S(2)}) %all-to-all-start.2) | async-done | bytes 786464 | tf_op jit(solution)/shard_map/all_to_all | solution.py:110
  159.4 4.4 %convolution_convert_fusion = bf16[1024,8,256]{0,2,1:T(8,128)(2,1)} fusion(bf16[8,192,256]{2,1,0:T(8,128)(2,1)} %all-to-all-done.2, f32[1024,384]{0,1:T(8,128)S(1)} %fusion.14), kind=kOutput, calls=%fused_computation | convolution fusion | flops 808583168 | bytes 6553600 | tf_op jit(solution)/shard_map/tf,sfd->tsd/dot_general | solution.py:134
  163.8 6.5 %copy.104 = bf16[1024,2048]{1,0:T(8,128)(2,1)} copy(bf16[1024,2048]{0,1:T(8,128)(2,1)} %bitcast.70) | data formatting | bytes 8388608 | tf_op jit(solution)/shard_map/reshape | solution.py:135
  170.3 141.7 %reduce-scatter.2.cloned.1.call-done = bf16[32,2048]{1,0:T(8,128)(2,1)} async-done(((bf16[1024,2048]{1,0:T(8,128)(2,1)}), bf16[32,2048]{1,0:T(8,128)(2,1)}) %reduce-scatter.2.cloned.1.call-update) | async-done | bytes 131088 | tf_op jit(solution)/shard_map/reduce_scatter | solution.py:136
  312.1 1.6 add_convert_fusion
  (42 shorter events, 0.4 us)
Async XLA Ops:
  6.5 4.7 %copy-start.7 = (f32[2]{0:T(128)S(1)}, f32[2]{0:T(128)}, u32[]{:S(2)}) copy-start(f32[2]{0:T(128)} %constant.50.clone) | copy-start | bytes 28
  20.3 1.3 copy-start
  21.7 2.1 copy-start.3
  62.9 1.4 copy-start.4
  62.9 1.4 copy-start.8
  62.9 5.5 %copy-start.9 = (f32[256]{0:T(256)S(1)}, f32[256]{0:T(256)}, u32[]{:S(2)}) copy-start(f32[256]{0:T(256)} %param.22) | copy-start | bytes 3076
  63.0 10.9 %copy-start.5 = (bf16[32,2048]{1,0:T(8,128)(2,1)S(1)}, bf16[32,2048]{1,0:T(8,128)(2,1)}, u32[]{:S(2)}) copy-start(bf16[32,2048]{1,0:T(8,128)(2,1)} %param.24) | copy-start | bytes 393220
  65.0 8.8 %all-to-all-start = ((f32[4,32,256]{2,1,0:T(8,128)}), f32[4,32,256]{2,1,0:T(8,128)S(1)}, u32[]{:S(2)}, u32[]{:S(2)}) async-start(f32[4,32,256]{2,1,0:T(8,128)} %bitcast.17), calls=%async_computation | async-start | bytes 262144 | tf_op jit(solution)/shard_map/all_to_all | solution.py:113
  68.3 82.4 %all-gather.4.cloned.1.call-start = ((), (), s32[]{:S(2)}) async-start(), calls=%async_computation.4 | async-start | bytes 4325376 | tf_op jit(solution)/shard_map/all_gather | solution.py:121
  73.9 3.3 %copy-start.6 = (f32[2048]{0:T(1024)S(1)}, f32[2048]{0:T(1024)}, u32[]{:S(2)}) copy-start(f32[2048]{0:T(1024)} %param.25) | copy-start | bytes 24580
  73.9 4.1 %copy-start.1 = (bf16[256,1536]{1,0:T(8,128)(2,1)S(1)}, bf16[256,1536]{1,0:T(8,128)(2,1)}, u32[]{:S(2)}) copy-start(bf16[256,1536]{1,0:T(8,128)(2,1)} %param.26) | copy-start | bytes 2359300
  77.2 1.2 copy-start.2
  130.0 29.3 %all-to-all-start.2 = ((bf16[8,192,256]{2,1,0:T(8,128)(2,1)}), bf16[8,192,256]{2,1,0:T(8,128)(2,1)}, u32[]{:S(2)}, u32[]{:S(2)}) async-start(bf16[8,192,256]{2,1,0:T(8,128)(2,1)} %bitcast.27), calls=%async_computation.2 | async-start | bytes 1572864 | tf_op jit(solution)/shard_map/all_to_all | solution.py:110
  134.2 177.8 %reduce-scatter.2.cloned.1.call-start = ((), (), s32[]{:S(2)}) async-start(), calls=%async_computation.5 | async-start | bytes 4325376 | tf_op jit(solution)/shard_map/reduce_scatter | solution.py:136
Sparse Core Ops, SparseCore 0:
  78.1 72.5 all-gather.3
  170.5 141.5 reduce-scatter.1
